TPU v7x, 512 devices: a 8x2x16 block of a 8x16x16 slice. The times are simulated.
512 devices in a mesh: grp: 2 (over y), ep: 16 (over z), tp: 16 (over x, core).
Axes of the slice: x: 8, y: 2, z: 16, core: 2. Of those that a mesh axis runs over, the one named last changes fastest.
The devices are a block of a 8x16x16 slice.
Arguments:
- tokens: bfloat16 [192, 2048], P('grp', 'ep'), parts along dimension 0, may hold values from -70 to 70
- first_gain: float32 [2048], replicated, may hold values from 0.1 to 1.9
- w_query: bfloat16 [2048, 2048], P('ep', 'tp'), may hold values from -0.125 to 0.125
- w_key: bfloat16 [2048, 2048], P('ep', 'tp'), may hold values from -0.125 to 0.125
- w_value: bfloat16 [2048, 4096], P('ep', 'tp'), may hold values from -0.125 to 0.125
- w_outgate: bfloat16 [2048, 4096], P('ep', 'tp'), may hold values from -0.125 to 0.125
- w_input: bfloat16 [2048, 16], replicated, may hold values from -0.125 to 0.125
- w_forget: bfloat16 [2048, 16], replicated, may hold values from -0.125 to 0.125
- input_bias: float32 [16], replicated, may hold values from -3 to 3
- forget_bias: float32 [16], replicated, may hold values from -2 to 5
- head_gain: float32 [4096], replicated, may hold values from 0.1 to 1.9
- w_project: bfloat16 [4096, 2048], P('tp', 'ep'), may hold values from -0.09375 to 0.09375
- cell_state: float32 [192, 16, 128, 256], P(('grp', 'ep'), 'tp'), parts along dimension 0, may hold values from -6 to 6
- norm_state: float32 [192, 16, 128], P(('grp', 'ep'), 'tp'), parts along dimension 0, may hold values from -6 to 6
- max_state: float32 [192, 16], P(('grp', 'ep'), 'tp'), parts along dimension 0, may hold values from -110 to 110
- second_gain: float32 [2048], replicated, may hold values from 0.1 to 1.9
- routes: int32 [192, 2], P('grp'), parts along dimension 0, may hold values from 0 to 15, all different within a row; in each aligned block of 6 rows (0 to 5, 6 to 11, ...) at most 2 rows name the same one
- route_weight: float32 [192, 2], P('grp'), parts along dimension 0, may hold values from 0.2 to 1
- expert_gate: bfloat16 [16, 2048, 4096], P('ep', None, 'tp'), may hold values from -0.125 to 0.125
- expert_up: bfloat16 [16, 2048, 4096], P('ep', None, 'tp'), may hold values from -0.125 to 0.125
- expert_down: bfloat16 [16, 4096, 2048], P('ep', 'tp'), may hold values from -0.09375 to 0.09375
Outputs:
- layer_out: bfloat16 [192, 2048], P('grp', 'ep'), parts along dimension 0
- new_cell: float32 [192, 16, 128, 256], P(('grp', 'ep'), 'tp'), parts along dimension 0
- new_norm: float32 [192, 16, 128], P(('grp', 'ep'), 'tp'), parts along dimension 0
- new_max: float32 [192, 16], P(('grp', 'ep'), 'tp'), parts along dimension 0
There are 2 independent parts, one for each index of `grp`. A program takes and returns all parts, laid end to end along the dimension named above; an argument that names none is the same for every part. Nothing has to cross between parts.
Inputs may be any that keep to these rules, and one draw needn't show every extreme that they name: `routes`: each sequence names 2 different experts. In each aligned block of 6 sequences no expert is named by more than 2 of them, a bound that some block reaches.
All inputs are finite; a program needn't handle non-finite values.
Results may differ from a plain program's by a relative error of at most 0.0065.
Values may be sent and summed in bfloat16 or wider, within the bound.
No kernel may reach another device: no remote copies, remote signals or barrier semaphores. Data moves between devices by JAX's collectives and lax.ppermute only.
A program may use at most 64 MiB of HBM per device.

v0:
```python
import jax
import jax.numpy as jnp
from jax import lax
from jax.sharding import PartitionSpec as P

EXP_DEV = 1
NORM_EPS = 1e-05
HEAD_EPS = 1e-06


def from_everyone(array, axis):
    peers = lax.axis_size(axis)
    return lax.all_to_all(
        jnp.broadcast_to(array[None], (peers, *array.shape)), axis, 0, 0, tiled=True
    )


def taken_together(array, axis):
    everything = from_everyone(array, axis)
    return jnp.sum(everything, axis=0)


def in_one(arrays, axis):
    ends = [0]
    for a in arrays:
        ends.append(ends[-1] + a.size)
    subtotal = taken_together(jnp.concatenate([a.ravel() for a in arrays]), axis)
    return tuple((subtotal[b:e].reshape(a.shape) for a, b, e in zip(arrays, ends, ends[1:])))


def cut_along(array, dim, peers):
    lengths = array.shape
    blocks = array.reshape(*lengths[:dim], peers, lengths[dim] // peers, *lengths[dim + 1 :])
    return jnp.moveaxis(blocks, dim, 0)


def summed_on_arrival(array, axis, dim):
    blocks = cut_along(array, dim, lax.axis_size(axis))
    arrived = lax.all_to_all(blocks, axis, split_axis=0, concat_axis=0, tiled=True)
    return arrived.astype(jnp.float32).sum(axis=0)


def summed_on_arrival_2(array, axis, dim):
    blocks = cut_along(array, dim, lax.axis_size(axis))
    arrived = lax.all_to_all(blocks, axis, split_axis=0, concat_axis=0, tiled=True)
    return arrived.sum(axis=0)


def side_by_side(arrays, axis, dim, along):
    ends, at = ([], 0)
    for a in arrays[:-1]:
        at += a.shape[along]
        ends.append(at)
    both = jnp.concatenate(arrays, axis=along)
    return tuple(jnp.split(summed_on_arrival_2(both, axis, dim), ends, axis=along))


def joined_along(blocks, dim):
    lengths = list(blocks.shape[1:])
    lengths[dim] *= blocks.shape[0]
    return jnp.moveaxis(blocks, 0, dim).reshape(lengths)


def gather_directly(array, axis, dim):
    return joined_along(from_everyone(array, axis), dim)


def gathered_total(array, axis):
    blocks = lax.all_gather(array, axis)
    return blocks.sum(axis=0)


def row_norm(stream_rows, gain_whole):
    col_count = stream_rows.shape[1]
    gain_cols = lax.dynamic_slice_in_dim(gain_whole, lax.axis_index("ep") * col_count, col_count, 0)
    values = stream_rows.astype(jnp.float32)
    totals, squares = in_one((jnp.sum(values, axis=1), jnp.sum(values * values, axis=1)), "ep")
    features = col_count * lax.axis_size("ep")
    row_mean = totals / features
    spread = squares / features - row_mean * row_mean
    inv_scale = lax.rsqrt(spread + NORM_EPS)
    return ((values - row_mean[:, None]) * inv_scale[:, None] * gain_cols).astype(jnp.bfloat16)


def expert_act(gate_sum, up_sum):
    return (jax.nn.silu(gate_sum) * up_sum).astype(jnp.bfloat16)


def scatter_slots(active, expert_down):
    slot_major = jnp.moveaxis(active, 1, 0)
    return summed_on_arrival(
        jnp.einsum(
            "pef,efd->ped", slot_major, expert_down, preferred_element_type=jnp.float32
        ).astype(jnp.bfloat16),
        "tp",
        0,
    ).astype(jnp.bfloat16)


def on_device(
    tokens,
    first_gain,
    w_query,
    w_key,
    w_value,
    w_outgate,
    w_input,
    w_forget,
    input_bias,
    forget_bias,
    head_gain,
    w_project,
    cell_state,
    norm_state,
    max_state,
    second_gain,
    routes,
    route_weight,
    expert_gate,
    expert_up,
    expert_down,
):
    blocks = lax.axis_size("ep")
    columns = tokens.shape[1]
    seq_total = tokens.shape[0]
    seq_local = seq_total // blocks
    heads_local = cell_state.shape[1]
    key_size = cell_state.shape[2]
    value_size = cell_state.shape[3]
    col_start = lax.axis_index("ep") * columns
    head_start = lax.axis_index("tp") * heads_local
    normed = row_norm(tokens, first_gain)
    input_cols = lax.dynamic_slice(w_input, (col_start, head_start), (columns, heads_local))
    forget_cols = lax.dynamic_slice(w_forget, (col_start, head_start), (columns, heads_local))

    def project_part(weight):
        return jnp.dot(normed, weight, preferred_element_type=jnp.float32)

    summed = side_by_side(
        (
            project_part(w_query),
            project_part(w_key),
            project_part(w_value),
            project_part(w_outgate),
            project_part(input_cols),
            project_part(forget_cols),
        ),
        "ep",
        0,
        1,
    )
    queries = summed[0].astype(jnp.bfloat16).reshape(seq_local, heads_local, key_size)
    key_rows = summed[1].astype(jnp.bfloat16).reshape(seq_local, heads_local, key_size)
    value_rows = summed[2].astype(jnp.bfloat16).reshape(seq_local, heads_local, value_size)
    outgate = summed[3].astype(jnp.bfloat16)
    input_pre = summed[4] + lax.dynamic_slice_in_dim(input_bias, head_start, heads_local, 0)
    forget_pre = summed[5] + lax.dynamic_slice_in_dim(forget_bias, head_start, heads_local, 0)
    carried = jax.nn.log_sigmoid(forget_pre) + max_state
    new_max = jnp.maximum(carried, input_pre)
    keep_old = jnp.exp(carried - new_max)
    admit_new = jnp.exp(input_pre - new_max)
    key_float = key_rows.astype(jnp.float32)
    value_float = value_rows.astype(jnp.float32)
    new_cell = (
        keep_old[:, :, None, None] * cell_state
        + admit_new[:, :, None, None] * key_float[:, :, :, None] * value_float[:, :, None, :]
    )
    new_norm = keep_old[:, :, None] * norm_state + admit_new[:, :, None] * key_float
    query_float = queries.astype(jnp.float32) * key_size ** (-0.5)
    readout = jnp.einsum("shk,shkv->shv", query_float, new_cell, precision=lax.Precision.HIGHEST)
    head_mean = jnp.mean(readout, axis=2, keepdims=True)
    centred = readout - head_mean
    head_var = jnp.mean(centred * centred, axis=2, keepdims=True)
    gains_here = lax.dynamic_slice_in_dim(
        head_gain, head_start * value_size, heads_local * value_size, 0
    )
    mixed_heads = (
        (centred * lax.rsqrt(head_var + HEAD_EPS)).reshape(seq_local, heads_local * value_size)
        * gains_here
        * jax.nn.sigmoid(outgate.astype(jnp.float32))
    ).astype(jnp.bfloat16)
    head_terms = jnp.dot(
        gather_directly(mixed_heads, "ep", 0), w_project, preferred_element_type=jnp.float32
    )
    mixer_out = gathered_total(head_terms, "tp")
    stream = (tokens.astype(jnp.float32) + mixer_out).astype(jnp.bfloat16)
    second_normed = row_norm(stream, second_gain)
    experts = blocks * EXP_DEV
    top_count = routes.shape[1]
    capacity = max(2, 2 * seq_local * top_count // experts)
    slot_count = blocks * capacity
    expert_ids = lax.broadcasted_iota(jnp.int32, (1, 1, experts), 2)
    matches = routes[:, :, None] == expert_ids
    routed = jnp.sum(matches.astype(jnp.int32), axis=1)
    combine = jnp.sum(jnp.where(matches, route_weight[:, :, None], 0.0), axis=1)
    running = (
        jnp.cumsum(routed.reshape(blocks, seq_local, experts), axis=1).reshape(seq_total, experts)
        - routed
    )
    block_ids = lax.broadcasted_iota(jnp.int32, (seq_total, experts), 0) // seq_local
    slot_of = block_ids * capacity + running
    slot_ids = lax.broadcasted_iota(jnp.int32, (experts, slot_count, seq_total), 1)
    placed = (slot_of.T[:, None, :] == slot_ids) & (routed.T[:, None, :] > 0)
    picker = placed.astype(jnp.bfloat16)
    weighted = jnp.where(placed, combine.T[:, None, :], 0.0)
    outbound = jnp.einsum(
        "eps,sd->epd", picker, second_normed, preferred_element_type=jnp.float32
    ).astype(jnp.bfloat16)
    arrived = lax.all_to_all(outbound, "ep", split_axis=0, concat_axis=2, tiled=True)
    gate_sum = jnp.einsum("end,edf->enf", arrived, expert_gate, preferred_element_type=jnp.float32)
    up_sum = jnp.einsum("end,edf->enf", arrived, expert_up, preferred_element_type=jnp.float32)
    active = expert_act(gate_sum, up_sum)
    share = scatter_slots(active, expert_down)
    back = lax.all_to_all(share, "ep", split_axis=2, concat_axis=1, tiled=True)
    every_slot = gather_directly(back, "tp", 0)
    moe_out = jnp.einsum(
        "eps,ped->sd", weighted, every_slot.astype(jnp.float32), precision=lax.Precision.HIGHEST
    )
    layer_out = (stream.astype(jnp.float32) + moe_out).astype(jnp.bfloat16)
    return (layer_out, new_cell, new_norm, new_max)


def solution(mesh):
    placed = (
        P("grp", "ep"),
        P(),
        P("ep", "tp"),
        P("ep", "tp"),
        P("ep", "tp"),
        P("ep", "tp"),
        P(),
        P(),
        P(),
        P(),
        P(),
        P("tp", "ep"),
        P(("grp", "ep"), "tp", None, None),
        P(("grp", "ep"), "tp", None),
        P(("grp", "ep"), "tp"),
        P(),
        P("grp", None),
        P("grp", None),
        P("ep", None, "tp"),
        P("ep", None, "tp"),
        P("ep", "tp", None),
    )
    return jax.shard_map(
        on_device,
        mesh=mesh,
        in_specs=placed,
        out_specs=(
            P("grp", "ep"),
            P(("grp", "ep"), "tp", None, None),
            P(("grp", "ep"), "tp", None),
            P(("grp", "ep"), "tp"),
        ),
        check_vma=False,
    )
```

profile of v0, /device:TPU:65, one launch (start us, length us, event | category | flops | bytes accessed | tf_op | source)
XLA Modules:
  0.0 232.7 jit_solution(2197950431508416456)
XLA Ops:
  0.6 0.9 convert_reduce_fusion.1
  1.7 0.6 broadcast_in_dim.26
  2.3 44.2 %all-to-all-start = ((f32[16,1,192]{2,1,0:T(1,128)}), f32[16,1,192]{2,1,0:T(1,128)S(1)}, u32[]{:S(2)}, u32[]{:S(2)}) async-start(f32[16,1,192]{2,1,0:T(1,128)} %broadcast_in_dim.26), calls=%async_computation | async-start | bytes 32768 | tf_op jit(solution)/shard_map/all_to_all | solution.py:13
  46.5 0.8 dynamic_slice.21
  47.3 10.4 %all-to-all-done = f32[16,1,192]{2,1,0:T(1,128)S(1)} async-done(((f32[16,1,192]{2,1,0:T(1,128)}), f32[16,1,192]{2,1,0:T(1,128)S(1)}, u32[]{:S(2)}, u32[]{:S(2)}) %all-to-all-start) | async-done | bytes 12320 | tf_op jit(solution)/shard_map/all_to_all | solution.py:13
  57.8 0.1 fusion.30
  57.9 0.9 fusion.46
  58.8 0.1 copy.110
  58.9 0.9 fusion.48
  59.8 0.1 copy.109
  59.9 0.6 copy-done.9
  60.6 0.1 fusion.71
  60.7 0.7 copy-done.10
  61.5 0.1 fusion.70
  61.6 0.1 copy.93
  61.8 0.1 copy.94
  61.9 0.6 copy-done.6
  62.5 0.1 fusion.73
  62.6 0.8 copy-done.7
  63.5 0.1 fusion.72
  63.6 0.9 concatenate.23
  64.5 4.1 %all-to-all-start.1 = ((f32[16,6,770]{2,1,0:T(8,128)}), f32[16,6,770]{2,1,0:T(8,128)S(1)}, u32[]{:S(2)}, u32[]{:S(2)}) async-start(f32[16,6,770]{2,1,0:T(8,128)} %concatenate.23), calls=%async_computation.1 | async-start | bytes 917504 | tf_op jit(solution)/shard_map/all_to_all | solution.py:45
  68.6 0.6 copy-done.15
  69.3 0.6 dynamic_slice.24
  69.9 0.6 dynamic_slice.25
  70.7 0.6 copy-done.11
  71.3 0.1 copy.96
  71.5 0.8 dynamic_slice.26
  72.3 17.0 %all-to-all-done.1 = f32[16,6,770]{2,1,0:T(8,128)S(1)} async-done(((f32[16,6,770]{2,1,0:T(8,128)}), f32[16,6,770]{2,1,0:T(8,128)S(1)}, u32[]{:S(2)}, u32[]{:S(2)}) %all-to-all-start.1) | async-done | bytes 295712 | tf_op jit(solution)/shard_map/all_to_all | solution.py:45
  89.3 1.5 exponential_reduce_fusion.1
  90.9 0.2 multiply_add_fusion
  91.1 0.5 fusion.9
  91.6 0.1 bitcast_reduce_fusion
  91.8 0.2 fusion.53
  92.0 0.6 broadcast_in_dim.27
  92.7 11.5 %all-to-all-start.2 = ((bf16[16,6,256]{2,1,0:T(8,128)(2,1)}), bf16[16,6,256]{2,1,0:T(8,128)(2,1)S(1)}, u32[]{:S(2)}, u32[]{:S(2)}) async-start(bf16[16,6,256]{2,1,0:T(8,128)(2,1)} %broadcast_in_dim.27), calls=%async_computation.2 | async-start | bytes 131072 | tf_op jit(solution)/shard_map/all_to_all | solution.py:13
  104.2 11.4 %all-to-all-done.2 = bf16[16,6,256]{2,1,0:T(8,128)(2,1)S(1)} async-done(((bf16[16,6,256]{2,1,0:T(8,128)(2,1)}), bf16[16,6,256]{2,1,0:T(8,128)(2,1)S(1)}, u32[]{:S(2)}, u32[]{:S(2)}) %all-to-all-start.2) | async-done | bytes 49184 | tf_op jit(solution)/shard_map/all_to_all | solution.py:13
  115.6 0.1 fusion.74
  115.7 22.3 %all-gather = f32[1536,128]{1,0:T(8,128)S(1)} all-gather(f32[96,128]{1,0:T(8,128)S(1)} %fusion.74), channel_id=2, replica_groups=mesh['grp'=2,'ep'=16,'tp'=16] {'tp'}, dimensions={0}, use_global_device_ids=true | all-gather | bytes 835584 | tf_op jit(solution)/shard_map/all_gather | solution.py:69
  138.1 0.1 convert_reduce_fusion
  138.3 0.6 broadcast_in_dim.32
  139.0 3.9 %all-to-all-start.3 = ((f32[16,1,192]{2,1,0:T(1,128)}), f32[16,1,192]{2,1,0:T(1,128)S(1)}, u32[]{:S(2)}, u32[]{:S(2)}) async-start(f32[16,1,192]{2,1,0:T(1,128)} %broadcast_in_dim.32), calls=%async_computation.3 | async-start | bytes 32768 | tf_op jit(solution)/shard_map/all_to_all | solution.py:13
  142.9 0.8 dynamic_slice.27
  143.7 10.2 %all-to-all-done.3 = f32[16,1,192]{2,1,0:T(1,128)S(1)} async-done(((f32[16,1,192]{2,1,0:T(1,128)}), f32[16,1,192]{2,1,0:T(1,128)S(1)}, u32[]{:S(2)}, u32[]{:S(2)}) %all-to-all-start.3) | async-done | bytes 12320 | tf_op jit(solution)/shard_map/all_to_all | solution.py:13
  154.0 0.3 convolution_convert_fusion.1
  154.3 14.6 %all_to_all.56 = bf16[16,32,128]{2,1,0:T(8,128)(2,1)S(1)} all-to-all(bf16[16,32,128]{2,1,0:T(8,128)(2,1)S(1)} %convolution_convert_fusion.1), channel_id=1, replica_groups=mesh['grp'=2,'ep'=16,'tp'=16] {'ep'}, dimensions={0} | all-to-all | bytes 262144 | tf_op jit(solution)/shard_map/all_to_all | solution.py:209
  168.9 0.3 fusion.7
  169.2 0.7 fusion
  169.9 0.1 reshape.205
  170.1 16.3 %all_to_all.57 = bf16[16,2,1,2048]{3,1,2,0:T(2,128)(2,1)S(1)} all-to-all(bf16[16,2,1,2048]{3,1,2,0:T(2,128)(2,1)S(1)} %bitcast.105), channel_id=1, replica_groups=mesh['grp'=2,'ep'=16,'tp'=16] {'tp'}, dimensions={0} | all-to-all | bytes 262144 | tf_op jit(solution)/shard_map/all_to_all | solution.py:39
  186.4 0.1 reduce_sum.134
  186.5 0.9 copy.101
  187.4 0.5 broadcast.140
  187.9 11.5 %reduce.12 = bf16[2048,2]{1,0:T(8,128)(2,1)S(1)} reduce(bf16[2048,1,2]{2,1,0:T(2,128)(2,1)S(1)} %bitcast.99, bf16[]{:T(256)} %broadcast.140), dimensions={1}, to_apply=%bitcast.86.reduce_sub_computation | reduce | bytes 16386
  199.4 0.6 reshape.218
  200.1 15.1 %all_to_all.58 = bf16[16,2,128]{2,1,0:T(2,128)(2,1)S(1)} all-to-all(bf16[16,2,128]{2,1,0:T(2,128)(2,1)S(1)} %reshape.218), channel_id=1, replica_groups=mesh['grp'=2,'ep'=16,'tp'=16] {'ep'}, dimensions={0} | all-to-all | bytes 16384 | tf_op jit(solution)/shard_map/all_to_all | solution.py:214
  215.1 1.2 reshape.219
  216.4 0.6 copy.102
  217.0 0.7 broadcast_in_dim.34
  217.7 4.7 %all-to-all-start.7 = ((bf16[16,2,16,128]{3,1,2,0:T(2,128)(2,1)}), bf16[16,2,16,128]{3,1,2,0:T(2,128)(2,1)S(1)}, u32[]{:S(2)}, u32[]{:S(2)}) async-start(bf16[16,2,16,128]{3,1,2,0:T(2,128)(2,1)} %broadcast_in_dim.34), calls=%async_computation.7 | async-start | bytes 262144 | tf_op jit(solution)/shard_map/all_to_all | solution.py:13
  222.4 0.6 copy.107
  223.2 0.6 copy.106
  223.7 7.9 %all-to-all-done.7 = bf16[16,2,16,128]{3,1,2,0:T(2,128)(2,1)S(1)} async-done(((bf16[16,2,16,128]{3,1,2,0:T(2,128)(2,1)}), bf16[16,2,16,128]{3,1,2,0:T(2,128)(2,1)S(1)}, u32[]{:S(2)}, u32[]{:S(2)}) %all-to-all-start.7) | async-done | bytes 131104 | tf_op jit(solution)/shard_map/all_to_all | solution.py:13
  231.7 1.0 fusion.2
  (62 shorter events, 1.5 us)
Async XLA Ops:
  0.6 168.6 %copy-start = (bf16[1,256,2048]{2,1,0:T(8,128)(2,1)S(1)}, bf16[1,256,2048]{2,1,0:T(8,128)(2,1)}, u32[]{:S(2)}) copy-start(bf16[1,256,2048]{2,1,0:T(8,128)(2,1)} %param.41) | copy-start | bytes 3145732
  2.3 55.4 %all-to-all-start = ((f32[16,1,192]{2,1,0:T(1,128)}), f32[16,1,192]{2,1,0:T(1,128)S(1)}, u32[]{:S(2)}, u32[]{:S(2)}) async-start(f32[16,1,192]{2,1,0:T(1,128)} %broadcast_in_dim.26), calls=%async_computation | async-start | bytes 32768 | tf_op jit(solution)/shard_map/all_to_all | solution.py:13
  46.5 11.3 %copy-start.5 = (bf16[96,128]{1,0:T(8,128)(2,1)S(1)}, bf16[96,128]{1,0:T(8,128)(2,1)}, u32[]{:S(2)}) copy-start(bf16[96,128]{1,0:T(8,128)(2,1)} %param.21) | copy-start | bytes 73732
  59.8 0.8 copy-start.9
  60.7 0.8 copy-start.10
  61.6 0.8 copy-start.6
  62.6 0.9 copy-start.7
  64.5 26.5 %copy-start.4 = (f32[6,1,128,256]{3,2,1,0:T(8,128)S(1)}, f32[6,1,128,256]{3,2,1,0:T(8,128)}, u32[]{:S(2)}) copy-start(f32[6,1,128,256]{3,2,1,0:T(8,128)} %param.33) | copy-start | bytes 2359300
  64.5 24.8 %all-to-all-start.1 = ((f32[16,6,770]{2,1,0:T(8,128)}), f32[16,6,770]{2,1,0:T(8,128)S(1)}, u32[]{:S(2)}, u32[]{:S(2)}) async-start(f32[16,6,770]{2,1,0:T(8,128)} %concatenate.23), calls=%async_computation.1 | async-start | bytes 917504 | tf_op jit(solution)/shard_map/all_to_all | solution.py:45
  68.6 0.7 copy-start.15
  69.3 0.7 copy-start.16
  69.9 0.7 copy-start.14
  70.6 0.7 copy-start.11
  91.1 46.9 %copy-start.1 = (f32[6,1,128,256]{3,2,1,0:T(8,128)}, f32[6,1,128,256]{3,2,1,0:T(8,128)S(1)}, u32[]{:S(2)}) copy-start(f32[6,1,128,256]{3,2,1,0:T(8,128)S(1)} %multiply_add_fusion) | copy-start | bytes 2359300
  92.7 22.9 %all-to-all-start.2 = ((bf16[16,6,256]{2,1,0:T(8,128)(2,1)}), bf16[16,6,256]{2,1,0:T(8,128)(2,1)S(1)}, u32[]{:S(2)}, u32[]{:S(2)}) async-start(bf16[16,6,256]{2,1,0:T(8,128)(2,1)} %broadcast_in_dim.27), calls=%async_computation.2 | async-start | bytes 131072 | tf_op jit(solution)/shard_map/all_to_all | solution.py:13
  104.2 11.4 %copy-start.8 = (bf16[256,128]{1,0:T(8,128)(2,1)S(1)}, bf16[256,128]{1,0:T(8,128)(2,1)}, u32[]{:S(2)}) copy-start(bf16[256,128]{1,0:T(8,128)(2,1)} %param.32) | copy-start | bytes 196612
  138.1 30.8 %copy-start.3 = (bf16[1,2048,256]{2,1,0:T(8,128)(2,1)S(1)}, bf16[1,2048,256]{2,1,0:T(8,128)(2,1)}, u32[]{:S(2)}) copy-start(bf16[1,2048,256]{2,1,0:T(8,128)(2,1)} %param.39) | copy-start | bytes 3145732
  138.2 31.0 %copy-start.2 = (bf16[1,2048,256]{2,1,0:T(8,128)(2,1)S(1)}, bf16[1,2048,256]{2,1,0:T(8,128)(2,1)}, u32[]{:S(2)}) copy-start(bf16[1,2048,256]{2,1,0:T(8,128)(2,1)} %param.40) | copy-start | bytes 3145732
  139.0 14.9 %all-to-all-start.3 = ((f32[16,1,192]{2,1,0:T(1,128)}), f32[16,1,192]{2,1,0:T(1,128)S(1)}, u32[]{:S(2)}, u32[]{:S(2)}) async-start(f32[16,1,192]{2,1,0:T(1,128)} %broadcast_in_dim.32), calls=%async_computation.3 | async-start | bytes 32768 | tf_op jit(solution)/shard_map/all_to_all | solution.py:13
  217.7 4.7 %copy-start.13 = (f32[96,2]{0,1:T(2,128)S(1)}, f32[96,2]{0,1:T(2,128)}, u32[]{:S(2)}) copy-start(f32[96,2]{0,1:T(2,128)} %param.38) | copy-start | bytes 2308
  217.7 13.9 %all-to-all-start.7 = ((bf16[16,2,16,128]{3,1,2,0:T(2,128)(2,1)}), bf16[16,2,16,128]{3,1,2,0:T(2,128)(2,1)S(1)}, u32[]{:S(2)}, u32[]{:S(2)}) async-start(bf16[16,2,16,128]{3,1,2,0:T(2,128)(2,1)} %broadcast_in_dim.34), calls=%async_computation.7 | async-start | bytes 262144 | tf_op jit(solution)/shard_map/all_to_all | solution.py:13
  222.4 0.7 copy-start.12
where the time goes:
time: 234 us; the launch traced here: 233 us
  starting transfers between devices  68.5 us (29%)
  blocking collectives  68.3 us (29%)
  waiting for transfers between devices  56.8 us (24%)
  local copies, waits for them, and re-layouts  17.4 us (7%)
  other arithmetic  15.6 us (7%)
  matrix products  5.14 us (2%)
    all_to_all x4, starting transfers between devices, from_everyone(): lax.all_to_all(jnp.broadcast_to(array[None], (peers, *array.shape)), axis...  64.3 us
    all_to_all x4, waiting for transfers between devices, from_everyone(): lax.all_to_all(jnp.broadcast_to(array[None], (peers, *array.shape)), axis...  39.9 us
    all_gather x1, blocking collectives, gathered_total(): blocks = lax.all_gather(array, axis)  22.3 us
    all_to_all x1, waiting for transfers between devices, summed_on_arrival_2(): lax.all_to_all(blocks, axis, split_axis=0, concat_axis=0, tiled=True)  17 us
    all_to_all x1, blocking collectives, summed_on_arrival(): lax.all_to_all(blocks, axis, split_axis=0, concat_axis=0, tiled=True)  16.3 us
    all_to_all x1, blocking collectives, on_device(): back = lax.all_to_all(share, 'ep', split_axis=2, concat_axis=1, tiled=True)  15.1 us
    all_to_all x1, blocking collectives, on_device(): lax.all_to_all(outbound, 'ep', split_axis=0, concat_axis=2, tiled=True)  14.6 us
    unnamed x1, other arithmetic  11.5 us
  transfers between devices with their start and end apart: 5, of which 5 were waited for; matrix products, arithmetic and copies ran while one was open for 2% of the time, Pallas kernels for 0%

commit v1 on v0

--- a/solution.py
+++ b/solution.py
@@ -206,7 +206,9 @@
     outbound = jnp.einsum(
         "eps,sd->epd", picker, second_normed, preferred_element_type=jnp.float32
     ).astype(jnp.bfloat16)
-    arrived = lax.all_to_all(outbound, "ep", split_axis=0, concat_axis=2, tiled=True)
+    pieces = jnp.split(outbound, lax.axis_size("ep"), axis=0)
+    received = lax.all_to_all(jnp.stack(pieces), "ep", 0, 0)
+    arrived = jnp.concatenate(received, axis=2)
     gate_sum = jnp.einsum("end,edf->enf", arrived, expert_gate, preferred_element_type=jnp.float32)
     up_sum = jnp.einsum("end,edf->enf", arrived, expert_up, preferred_element_type=jnp.float32)
     active = expert_act(gate_sum, up_sum)

time: 234 us -> 234 us (level)
    unnamed x40 -> x55, local copies, waits for them, and re-layouts: 7.97 us -> 8.09 us
where the time goes in v1:
time: 234 us; the launch traced here: 233 us
  starting transfers between devices  68.5 us (29%)
  blocking collectives  68.4 us (29%)
  waiting for transfers between devices  56.8 us (24%)
  local copies, waits for them, and re-layouts  17.5 us (7%)
  other arithmetic  15.6 us (7%)
  matrix products  5.14 us (2%)
    all_to_all x4, starting transfers between devices, from_everyone(): lax.all_to_all(jnp.broadcast_to(array[None], (peers, *array.shape)), axis...  64.3 us
    all_to_all x4, waiting for transfers between devices, from_everyone(): lax.all_to_all(jnp.broadcast_to(array[None], (peers, *array.shape)), axis...  39.9 us
    all_gather x1, blocking collectives, gathered_total(): blocks = lax.all_gather(array, axis)  22.3 us
    all_to_all x1, waiting for transfers between devices, summed_on_arrival_2(): lax.all_to_all(blocks, axis, split_axis=0, concat_axis=0, tiled=True)  17 us
    all_to_all x1, blocking collectives, summed_on_arrival(): lax.all_to_all(blocks, axis, split_axis=0, concat_axis=0, tiled=True)  16.3 us
    all_to_all x1, blocking collectives, on_device(): back = lax.all_to_all(share, 'ep', split_axis=2, concat_axis=1, tiled=True)  15.1 us
    all_to_all x1, blocking collectives, on_device(): received = lax.all_to_all(jnp.stack(pieces), 'ep', 0, 0)  14.7 us
    unnamed x1, other arithmetic  11.5 us
  transfers between devices with their start and end apart: 5, of which 5 were waited for; matrix products, arithmetic and copies ran while one was open for 2% of the time, Pallas kernels for 0%

profile of v1, /device:TPU:65, one launch (start us, length us, event | category | flops | bytes accessed | tf_op | source)
XLA Modules:
  0.0 233.0 jit_solution(11145311257155469580)
XLA Ops:
  0.6 0.9 convert_reduce_fusion.1
  1.7 0.6 broadcast_in_dim.26
  2.3 44.2 %all-to-all-start = ((f32[16,1,192]{2,1,0:T(1,128)}), f32[16,1,192]{2,1,0:T(1,128)S(1)}, u32[]{:S(2)}, u32[]{:S(2)}) async-start(f32[16,1,192]{2,1,0:T(1,128)} %broadcast_in_dim.26), calls=%async_computation | async-start | bytes 32768 | tf_op jit(solution)/shard_map/all_to_all | solution.py:13
  46.5 0.8 dynamic_slice.21
  47.3 10.4 %all-to-all-done = f32[16,1,192]{2,1,0:T(1,128)S(1)} async-done(((f32[16,1,192]{2,1,0:T(1,128)}), f32[16,1,192]{2,1,0:T(1,128)S(1)}, u32[]{:S(2)}, u32[]{:S(2)}) %all-to-all-start) | async-done | bytes 12320 | tf_op jit(solution)/shard_map/all_to_all | solution.py:13
  57.8 0.1 fusion.30
  57.9 0.9 fusion.46
  58.8 0.1 copy.110
  58.9 0.9 fusion.48
  59.8 0.1 copy.109
  59.9 0.6 copy-done.9
  60.6 0.1 fusion.71
  60.7 0.7 copy-done.10
  61.5 0.1 fusion.70
  61.6 0.1 copy.93
  61.8 0.1 copy.94
  61.9 0.6 copy-done.6
  62.5 0.1 fusion.73
  62.6 0.8 copy-done.7
  63.5 0.1 fusion.72
  63.6 0.9 concatenate.23
  64.5 4.1 %all-to-all-start.1 = ((f32[16,6,770]{2,1,0:T(8,128)}), f32[16,6,770]{2,1,0:T(8,128)S(1)}, u32[]{:S(2)}, u32[]{:S(2)}) async-start(f32[16,6,770]{2,1,0:T(8,128)} %concatenate.23), calls=%async_computation.1 | async-start | bytes 917504 | tf_op jit(solution)/shard_map/all_to_all | solution.py:45
  68.6 0.6 copy-done.15
  69.3 0.6 dynamic_slice.24
  69.9 0.6 dynamic_slice.25
  70.7 0.6 copy-done.11
  71.3 0.1 copy.96
  71.5 0.8 dynamic_slice.26
  72.3 17.0 %all-to-all-done.1 = f32[16,6,770]{2,1,0:T(8,128)S(1)} async-done(((f32[16,6,770]{2,1,0:T(8,128)}), f32[16,6,770]{2,1,0:T(8,128)S(1)}, u32[]{:S(2)}, u32[]{:S(2)}) %all-to-all-start.1) | async-done | bytes 295712 | tf_op jit(solution)/shard_map/all_to_all | solution.py:45
  89.3 1.5 exponential_reduce_fusion.1
  90.9 0.2 multiply_add_fusion
  91.1 0.5 fusion.9
  91.6 0.1 bitcast_reduce_fusion
  91.8 0.2 fusion.53
  92.0 0.6 broadcast_in_dim.27
  92.7 11.5 %all-to-all-start.2 = ((bf16[16,6,256]{2,1,0:T(8,128)(2,1)}), bf16[16,6,256]{2,1,0:T(8,128)(2,1)S(1)}, u32[]{:S(2)}, u32[]{:S(2)}) async-start(bf16[16,6,256]{2,1,0:T(8,128)(2,1)} %broadcast_in_dim.27), calls=%async_computation.2 | async-start | bytes 131072 | tf_op jit(solution)/shard_map/all_to_all | solution.py:13
  104.2 11.4 %all-to-all-done.2 = bf16[16,6,256]{2,1,0:T(8,128)(2,1)S(1)} async-done(((bf16[16,6,256]{2,1,0:T(8,128)(2,1)}), bf16[16,6,256]{2,1,0:T(8,128)(2,1)S(1)}, u32[]{:S(2)}, u32[]{:S(2)}) %all-to-all-start.2) | async-done | bytes 49184 | tf_op jit(solution)/shard_map/all_to_all | solution.py:13
  115.6 0.1 fusion.74
  115.7 22.3 %all-gather = f32[1536,128]{1,0:T(8,128)S(1)} all-gather(f32[96,128]{1,0:T(8,128)S(1)} %fusion.74), channel_id=2, replica_groups=mesh['grp'=2,'ep'=16,'tp'=16] {'tp'}, dimensions={0}, use_global_device_ids=true | all-gather | bytes 835584 | tf_op jit(solution)/shard_map/all_gather | solution.py:69
  138.1 0.1 convert_reduce_fusion
  138.3 0.6 broadcast_in_dim.32
  138.9 3.9 %all-to-all-start.3 = ((f32[16,1,192]{2,1,0:T(1,128)}), f32[16,1,192]{2,1,0:T(1,128)S(1)}, u32[]{:S(2)}, u32[]{:S(2)}) async-start(f32[16,1,192]{2,1,0:T(1,128)} %broadcast_in_dim.32), calls=%async_computation.3 | async-start | bytes 32768 | tf_op jit(solution)/shard_map/all_to_all | solution.py:13
  142.9 0.8 dynamic_slice.27
  143.7 10.2 %all-to-all-done.3 = f32[16,1,192]{2,1,0:T(1,128)S(1)} async-done(((f32[16,1,192]{2,1,0:T(1,128)}), f32[16,1,192]{2,1,0:T(1,128)S(1)}, u32[]{:S(2)}, u32[]{:S(2)}) %all-to-all-start.3) | async-done | bytes 12320 | tf_op jit(solution)/shard_map/all_to_all | solution.py:13
  154.0 0.3 convolution_convert_fusion.1
  154.5 14.7 %all_to_all.46 = bf16[16,1,32,128]{3,2,1,0:T(8,128)(2,1)S(1)} all-to-all(bf16[16,1,32,128]{3,2,1,0:T(8,128)(2,1)S(1)} %constant_dynamic-update-slice_fusion), channel_id=1, replica_groups=mesh['grp'=2,'ep'=16,'tp'=16] {'ep'}, dimensions={0} | all-to-all | bytes 262144 | tf_op jit(solution)/shard_map/all_to_all | solution.py:210
  169.3 0.3 fusion.7
  169.5 0.7 fusion
  170.3 0.1 reshape.210
  170.4 16.3 %all_to_all.47 = bf16[16,2,1,2048]{3,1,2,0:T(2,128)(2,1)S(1)} all-to-all(bf16[16,2,1,2048]{3,1,2,0:T(2,128)(2,1)S(1)} %bitcast.167), channel_id=1, replica_groups=mesh['grp'=2,'ep'=16,'tp'=16] {'tp'}, dimensions={0} | all-to-all | bytes 262144 | tf_op jit(solution)/shard_map/all_to_all | solution.py:39
  186.7 0.1 reduce_sum.134
  186.8 0.9 copy.101
  187.7 0.5 broadcast.140
  188.2 11.5 %reduce.12 = bf16[2048,2]{1,0:T(8,128)(2,1)S(1)} reduce(bf16[2048,1,2]{2,1,0:T(2,128)(2,1)S(1)} %bitcast.161, bf16[]{:T(256)} %broadcast.140), dimensions={1}, to_apply=%bitcast.148.reduce_sub_computation | reduce | bytes 16386
  199.7 0.6 reshape.223
  200.4 15.1 %all_to_all.48 = bf16[16,2,128]{2,1,0:T(2,128)(2,1)S(1)} all-to-all(bf16[16,2,128]{2,1,0:T(2,128)(2,1)S(1)} %reshape.223), channel_id=1, replica_groups=mesh['grp'=2,'ep'=16,'tp'=16] {'ep'}, dimensions={0} | all-to-all | bytes 16384 | tf_op jit(solution)/shard_map/all_to_all | solution.py:216
  215.5 1.2 reshape.224
  216.7 0.6 copy.102
  217.3 0.7 broadcast_in_dim.34
  218.0 4.7 %all-to-all-start.7 = ((bf16[16,2,16,128]{3,1,2,0:T(2,128)(2,1)}), bf16[16,2,16,128]{3,1,2,0:T(2,128)(2,1)S(1)}, u32[]{:S(2)}, u32[]{:S(2)}) async-start(bf16[16,2,16,128]{3,1,2,0:T(2,128)(2,1)} %broadcast_in_dim.34), calls=%async_computation.7 | async-start | bytes 262144 | tf_op jit(solution)/shard_map/all_to_all | solution.py:13
  222.7 0.6 copy.107
  223.5 0.6 copy.106
  224.1 7.9 %all-to-all-done.7 = bf16[16,2,16,128]{3,1,2,0:T(2,128)(2,1)S(1)} async-done(((bf16[16,2,16,128]{3,1,2,0:T(2,128)(2,1)}), bf16[16,2,16,128]{3,1,2,0:T(2,128)(2,1)S(1)}, u32[]{:S(2)}, u32[]{:S(2)}) %all-to-all-start.7) | async-done | bytes 131104 | tf_op jit(solution)/shard_map/all_to_all | solution.py:13
  232.1 1.0 fusion.2
  (78 shorter events, 1.7 us)
Async XLA Ops:
  0.6 168.9 %copy-start = (bf16[1,256,2048]{2,1,0:T(8,128)(2,1)S(1)}, bf16[1,256,2048]{2,1,0:T(8,128)(2,1)}, u32[]{:S(2)}) copy-start(bf16[1,256,2048]{2,1,0:T(8,128)(2,1)} %param.41) | copy-start | bytes 3145732
  2.3 55.4 %all-to-all-start = ((f32[16,1,192]{2,1,0:T(1,128)}), f32[16,1,192]{2,1,0:T(1,128)S(1)}, u32[]{:S(2)}, u32[]{:S(2)}) async-start(f32[16,1,192]{2,1,0:T(1,128)} %broadcast_in_dim.26), calls=%async_computation | async-start | bytes 32768 | tf_op jit(solution)/shard_map/all_to_all | solution.py:13
  46.5 11.3 %copy-start.5 = (bf16[96,128]{1,0:T(8,128)(2,1)S(1)}, bf16[96,128]{1,0:T(8,128)(2,1)}, u32[]{:S(2)}) copy-start(bf16[96,128]{1,0:T(8,128)(2,1)} %param.21) | copy-start | bytes 73732
  59.8 0.8 copy-start.9
  60.7 0.8 copy-start.10
  61.6 0.8 copy-start.6
  62.6 0.9 copy-start.7
  64.5 26.5 %copy-start.4 = (f32[6,1,128,256]{3,2,1,0:T(8,128)S(1)}, f32[6,1,128,256]{3,2,1,0:T(8,128)}, u32[]{:S(2)}) copy-start(f32[6,1,128,256]{3,2,1,0:T(8,128)} %param.33) | copy-start | bytes 2359300
  64.5 24.8 %all-to-all-start.1 = ((f32[16,6,770]{2,1,0:T(8,128)}), f32[16,6,770]{2,1,0:T(8,128)S(1)}, u32[]{:S(2)}, u32[]{:S(2)}) async-start(f32[16,6,770]{2,1,0:T(8,128)} %concatenate.23), calls=%async_computation.1 | async-start | bytes 917504 | tf_op jit(solution)/shard_map/all_to_all | solution.py:45
  68.6 0.7 copy-start.15
  69.3 0.7 copy-start.16
  69.9 0.7 copy-start.14
  70.6 0.7 copy-start.11
  91.1 46.9 %copy-start.1 = (f32[6,1,128,256]{3,2,1,0:T(8,128)}, f32[6,1,128,256]{3,2,1,0:T(8,128)S(1)}, u32[]{:S(2)}) copy-start(f32[6,1,128,256]{3,2,1,0:T(8,128)S(1)} %multiply_add_fusion) | copy-start | bytes 2359300
  92.7 22.9 %all-to-all-start.2 = ((bf16[16,6,256]{2,1,0:T(8,128)(2,1)}), bf16[16,6,256]{2,1,0:T(8,128)(2,1)S(1)}, u32[]{:S(2)}, u32[]{:S(2)}) async-start(bf16[16,6,256]{2,1,0:T(8,128)(2,1)} %broadcast_in_dim.27), calls=%async_computation.2 | async-start | bytes 131072 | tf_op jit(solution)/shard_map/all_to_all | solution.py:13
  104.2 11.4 %copy-start.8 = (bf16[256,128]{1,0:T(8,128)(2,1)S(1)}, bf16[256,128]{1,0:T(8,128)(2,1)}, u32[]{:S(2)}) copy-start(bf16[256,128]{1,0:T(8,128)(2,1)} %param.32) | copy-start | bytes 196612
  138.1 31.2 %copy-start.3 = (bf16[1,2048,256]{2,1,0:T(8,128)(2,1)S(1)}, bf16[1,2048,256]{2,1,0:T(8,128)(2,1)}, u32[]{:S(2)}) copy-start(bf16[1,2048,256]{2,1,0:T(8,128)(2,1)} %param.39) | copy-start | bytes 3145732
  138.9 14.9 %all-to-all-start.3 = ((f32[16,1,192]{2,1,0:T(1,128)}), f32[16,1,192]{2,1,0:T(1,128)S(1)}, u32[]{:S(2)}, u32[]{:S(2)}) async-start(f32[16,1,192]{2,1,0:T(1,128)} %broadcast_in_dim.32), calls=%async_computation.3 | async-start | bytes 32768 | tf_op jit(solution)/shard_map/all_to_all | solution.py:13
  154.2 15.3 %copy-start.2 = (bf16[1,2048,256]{2,1,0:T(8,128)(2,1)S(1)}, bf16[1,2048,256]{2,1,0:T(8,128)(2,1)}, u32[]{:S(2)}) copy-start(bf16[1,2048,256]{2,1,0:T(8,128)(2,1)} %param.40) | copy-start | bytes 3145732
  218.0 4.7 %copy-start.13 = (f32[96,2]{0,1:T(2,128)S(1)}, f32[96,2]{0,1:T(2,128)}, u32[]{:S(2)}) copy-start(f32[96,2]{0,1:T(2,128)} %param.38) | copy-start | bytes 2308
  218.0 13.9 %all-to-all-start.7 = ((bf16[16,2,16,128]{3,1,2,0:T(2,128)(2,1)}), bf16[16,2,16,128]{3,1,2,0:T(2,128)(2,1)S(1)}, u32[]{:S(2)}, u32[]{:S(2)}) async-start(bf16[16,2,16,128]{3,1,2,0:T(2,128)(2,1)} %broadcast_in_dim.34), calls=%async_computation.7 | async-start | bytes 262144 | tf_op jit(solution)/shard_map/all_to_all | solution.py:13
  222.7 0.7 copy-start.12
